TPU v7x, 256 devices: a whole 4x4x8 slice. The times are simulated.
256 devices in a mesh: sp: 32 (over z, x), tp: 8 (over y, core).
Axes of the slice: x: 4, y: 4, z: 8, core: 2. Of those that a mesh axis runs over, the one named last changes fastest.
Arguments:
- tokens: bfloat16 [24576, 2048], P(('sp', 'tp')), may hold values from -6 to 6
- in_gain: float32 [2048], replicated, may hold values from 0.1 to 1.9
- w_query: bfloat16 [2048, 1024], P(None, 'tp'), may hold values from -0.125 to 0.125
- w_key: bfloat16 [2048, 1024], P(None, 'tp'), may hold values from -0.125 to 0.125
- w_value: bfloat16 [2048, 2048], P(None, 'tp'), may hold values from -0.125 to 0.125
- w_input_gate: bfloat16 [2048, 8], replicated, may hold values from -8 to 8
- w_forget_gate: bfloat16 [2048, 8], replicated, may hold values from -0.125 to 0.125
- forget_bias: float32 [8], replicated
- forget_extra: float32 [24576, 8], P('sp', 'tp'), may hold values from -2 to 0
- w_conv_gate: bfloat16 [2048, 2048], P(None, 'tp'), may hold values from -0.125 to 0.125
- w_conv_left: bfloat16 [2048, 2048], P(None, 'tp'), may hold values from -0.125 to 0.125
- w_conv_right: bfloat16 [2048, 2048], P(None, 'tp'), may hold values from -0.125 to 0.125
- conv_taps: float32 [3, 2048], replicated, may hold values from -3.5 to 3.5
- first_memory: float32 [8, 128, 256], P('tp'), may hold values from -5120 to 5120
- first_norm: float32 [8, 128], P('tp'), may hold values from -5120 to 5120
- w_out_memory: bfloat16 [2048, 2048], P('tp'), may hold values from -0.09375 to 0.09375
- w_out_conv: bfloat16 [2048, 2048], P('tp'), may hold values from -0.09375 to 0.09375
Outputs:
- mixed: bfloat16 [24576, 2048], P(('sp', 'tp'))
All inputs are finite; a program needn't handle non-finite values.
Results may differ from a plain program's by a relative error of at most 0.015.
The roundings to bfloat16 on the way count: a program that leaves them out, or rounds other values in their place, can miss the bound.
Values may be sent and summed in bfloat16 or wider, within the bound.
A program may use at most 64 MiB of HBM per device.

v0:
```python
import jax
import jax.numpy as jnp
from jax import lax
from jax.sharding import Mesh
from jax.sharding import PartitionSpec as P

KEY_DIM = 128
VALUE_DIM = 256
TAPS = 3
V_WIDTH = 2048
SP = ("sp_0", "sp_1")
SP_TP = ("sp_0", "sp_1", "tp")
epsilon = 1e-06
very_negative = -1e30
highest = lax.Precision.HIGHEST


def from_behind(block, axis, distance):
    devices = range(lax.axis_size(axis))
    route = [(i - distance, i) for i in devices if i - distance in devices]
    return lax.ppermute(block, axis, route)


def filled_with(x, identity):
    return jax.tree.map(
        lambda part, zero: jnp.zeros_like(part) + jnp.asarray(zero, part.dtype), x, identity
    )


def collected_together(x, axis):
    leaves = jax.tree.leaves(x)
    sequence = sorted(range(len(leaves)), key=lambda k: -leaves[k].size)
    width = (1, *leaves[sequence[0]].shape)[-1]
    lines = [
        jnp.pad(leaves[k].reshape(-1), (0, -leaves[k].size % width)).reshape(-1, width)
        for k in sequence
    ]
    both, at, found = (lax.all_gather(jnp.concatenate(lines), axis), 0, {})
    for k, line in zip(sequence, lines):
        slab = both[:, at : at + len(line)].reshape(len(both), -1)
        found[k] = slab[:, : leaves[k].size].reshape(-1, *leaves[k].shape)
        at += len(line)
    numbers = iter(range(len(leaves)))
    return jax.tree.map(lambda _: found[next(numbers)], x)


def entering(x, axes, combine, identity):
    before = start = filled_with(x, identity)
    running = x
    for axis in reversed(axes):
        size, here = (lax.axis_size(axis), lax.axis_index(axis))
        pieces = collected_together(running, axis)
        inside, running = (start, start)
        for k in range(size):
            passed = k < here
            running = combine(running, jax.tree.map(lambda part: part[k], pieces))
            inside = jax.tree.map(lambda new, old: jnp.where(passed, new, old), running, inside)
        before = combine(inside, before)
    return before


def rounded(values):
    return lax.optimization_barrier(values.astype(jnp.bfloat16)).astype(jnp.float32)


def join_states(earlier, later):
    decay_early, max_early, memory_early, norm_early = earlier
    decay_late, max_late, memory_late, norm_late = later
    joined_max = jnp.maximum(max_early + decay_late, max_late)
    scale_early = jnp.exp(max_early + decay_late - joined_max)
    scale_late = jnp.exp(max_late - joined_max)
    joined_memory = (
        scale_early[:, None, None] * memory_early + scale_late[:, None, None] * memory_late
    )
    joined_norm = scale_early[:, None] * norm_early + scale_late[:, None] * norm_late
    return (decay_early + decay_late, joined_max, joined_memory, joined_norm)


def per_device(
    tokens,
    in_gain,
    w_query,
    w_key,
    w_value,
    w_input_gate,
    w_forget_gate,
    forget_bias,
    forget_extra,
    w_conv_gate,
    w_conv_left,
    w_conv_right,
    conv_taps,
    first_memory,
    first_norm,
    w_out_memory,
    w_out_conv,
):
    heads_here = w_query.shape[1] // KEY_DIM
    query_width = heads_here * KEY_DIM
    value_width = heads_here * VALUE_DIM
    channels = w_conv_gate.shape[1]
    head_first = lax.axis_index("tp") * heads_here
    channel_first = lax.axis_index("tp") * channels
    input_gate = lax.dynamic_slice_in_dim(w_input_gate, head_first, heads_here, 1)
    forget_gate = lax.dynamic_slice_in_dim(w_forget_gate, head_first, heads_here, 1)
    bias_here = lax.dynamic_slice_in_dim(forget_bias, head_first, heads_here, 0)
    taps_here = lax.dynamic_slice_in_dim(conv_taps, channel_first, channels, 1)
    token_rows = tokens.astype(jnp.float32)
    scale_rows = lax.rsqrt(jnp.mean(token_rows * token_rows, axis=1, keepdims=True) + epsilon)
    normed = (token_rows * scale_rows * in_gain).astype(jnp.bfloat16)
    sub_rows = lax.all_gather(normed, "tp", axis=0, tiled=True)
    pieces = [
        jnp.dot(sub_rows, weight, preferred_element_type=jnp.float32)
        for weight in (
            w_query,
            w_key,
            w_value,
            w_conv_gate,
            w_conv_left,
            w_conv_right,
            input_gate,
            forget_gate,
        )
    ]
    projected = jnp.concatenate(pieces, axis=1)
    row_count = projected.shape[0]
    offset_value = 2 * query_width
    offset_conv = offset_value + value_width
    offset_gate = offset_conv + 3 * channels
    query_rows = (
        projected[:, 0:query_width].astype(jnp.bfloat16).reshape(row_count, heads_here, KEY_DIM)
    )
    key_rows = (
        projected[:, query_width:offset_value]
        .astype(jnp.bfloat16)
        .reshape(row_count, heads_here, KEY_DIM)
    )
    value_rows = (
        projected[:, offset_value:offset_conv]
        .astype(jnp.bfloat16)
        .reshape(row_count, heads_here, VALUE_DIM)
    )
    conv_gate = rounded(projected[:, offset_conv : offset_conv + channels])
    conv_left = rounded(projected[:, offset_conv + channels : offset_conv + 2 * channels])
    conv_right = rounded(projected[:, offset_conv + 2 * channels : offset_gate])
    in_pre = projected[:, offset_gate : offset_gate + heads_here]
    forget_pre = projected[:, offset_gate + heads_here : offset_gate + 2 * heads_here] + bias_here
    log_forget = jax.nn.log_sigmoid(forget_pre) + forget_extra
    cumulative = jnp.cumsum(log_forget, axis=0)
    decay_total = cumulative[row_count - 1]
    weight_log = decay_total[None, :] - cumulative + in_pre
    block_max = jnp.max(weight_log, axis=0)
    keyed = key_rows.astype(jnp.float32) * jnp.exp(weight_log - block_max[None, :])[:, :, None]
    block_norm = jnp.sum(keyed, axis=0)
    block_memory = jnp.einsum(
        "shd,shv->hdv", keyed.astype(jnp.bfloat16), value_rows, preferred_element_type=jnp.float32
    )
    product = (conv_left * conv_right).astype(jnp.bfloat16)
    edge_rows = product[row_count - (TAPS - 1) :]
    before_rows = from_behind(edge_rows, SP, 1)
    prior_decay, prior_max, prior_memory, prior_norm = entering(
        (decay_total, block_max, block_memory, block_norm),
        SP,
        join_states,
        (
            jnp.zeros_like(decay_total),
            jnp.full_like(block_max, very_negative),
            jnp.zeros_like(block_memory),
            jnp.zeros_like(block_norm),
        ),
    )
    enter_max = jnp.maximum(prior_max, prior_decay)
    from_prior = jnp.exp(prior_max - enter_max)
    from_first = jnp.exp(prior_decay - enter_max)
    carry_memory = (
        from_prior[:, None, None] * prior_memory + from_first[:, None, None] * first_memory
    )
    carry_norm = from_prior[:, None] * prior_norm + from_first[:, None] * first_norm
    query_scale = KEY_DIM ** (-0.5)
    row_ids = lax.iota(jnp.int32, row_count)
    causal = row_ids[:, None] >= row_ids[None, :]
    cum_heads = cumulative.T
    log_gap = cum_heads[:, :, None] - cum_heads[:, None, :] + in_pre.T[:, None, :]
    log_gap = jnp.where(causal[None], log_gap, -jnp.inf)
    inter_log = cum_heads + enter_max[:, None]
    row_max = jnp.maximum(inter_log, jnp.max(log_gap, axis=2))
    raw_scores = (
        jnp.einsum("thd,shd->hts", query_rows, key_rows, preferred_element_type=jnp.float32)
        * query_scale
    )
    mixing = raw_scores * jnp.exp(log_gap - row_max[:, :, None])
    carried = jnp.exp(inter_log - row_max).T
    scaled_query = query_rows.astype(jnp.float32) * query_scale
    from_values = jnp.einsum(
        "hts,shv->thv", mixing.astype(jnp.bfloat16), value_rows, preferred_element_type=jnp.float32
    )
    from_memory = jnp.einsum("thd,hdv->thv", scaled_query, carry_memory, precision=highest)
    from_norm = jnp.einsum("thd,hd->th", scaled_query, carry_norm, precision=highest)
    numerator = from_values + carried[:, :, None] * from_memory
    denominator = jnp.sum(mixing, axis=2).T + carried * from_norm
    memory_out = numerator / jnp.maximum(jnp.abs(denominator), 1.0)[:, :, None]
    local_squares = jnp.sum(memory_out * memory_out, axis=(1, 2))
    row_total = lax.psum(local_squares, "tp")
    row_scale = lax.rsqrt(row_total / V_WIDTH + epsilon)
    heads_out = memory_out * row_scale[:, None, None]
    heads_out = heads_out.reshape(row_count, value_width).astype(jnp.bfloat16)
    padded = jnp.concatenate([before_rows, product], axis=0).astype(jnp.float32)
    filtered = taps_here[0][None, :] * padded[0:row_count]
    for tap_index in range(1, TAPS):
        filtered = (
            filtered + taps_here[tap_index][None, :] * padded[tap_index : tap_index + row_count]
        )
    conv_branch = (conv_gate * filtered).astype(jnp.bfloat16)
    return lax.psum_scatter(
        (
            jnp.dot(heads_out, w_out_memory, preferred_element_type=jnp.float32)
            + jnp.dot(conv_branch, w_out_conv, preferred_element_type=jnp.float32)
        ).astype(jnp.bfloat16),
        "tp",
        scatter_dimension=0,
        tiled=True,
    )


def solution(mesh):
    split = Mesh(mesh.devices.reshape(8, 4, mesh.shape["tp"]), ("sp_0", "sp_1", "tp"))
    placed = (
        P(SP_TP, None),
        P(),
        P(None, "tp"),
        P(None, "tp"),
        P(None, "tp"),
        P(),
        P(),
        P(),
        P(SP, "tp"),
        P(None, "tp"),
        P(None, "tp"),
        P(None, "tp"),
        P(),
        P("tp", None, None),
        P("tp", None),
        P("tp", None),
        P("tp", None),
    )
    return jax.shard_map(
        per_device, mesh=split, in_specs=placed, out_specs=P(SP_TP, None), check_vma=False
    )
```

profile of v0, /device:TPU:2, one launch (start us, length us, event | category | flops | bytes accessed | tf_op | source)
XLA Modules:
  0.0 207.4 jit_solution(9044216374947095805)
XLA Ops:
  6.5 1.3 fusion.4
  7.8 1.9 fusion.6
  9.8 1.2 dynamic_slice.13
  11.0 0.9 constant_dynamic-slice_fusion
  11.9 31.2 %all-gather.7.cloned.1.call-done = bf16[768,2048]{1,0:T(8,128)(2,1)} async-done(((bf16[96,2048]{1,0:T(8,128)(2,1)}), bf16[768,2048]{1,0:T(8,128)(2,1)}) %all-gather.7.cloned.1.call-update) | async-done | bytes 3145744 | tf_op jit(solution)/shard_map/all_gather | solution.py:111
  43.1 2.8 %convolution_reduce_fusion.1 = f32[768]{0:T(1024)S(1)} fusion(bf16[768,2048]{1,0:T(8,128)(2,1)} %all-gather.7.cloned.1.call-done, bf16[2048,8]{0,1:T(8,128)(2,1)} %param.23, s32[]{:T(128)S(6)} %select_n.346), kind=kOutput, calls=%fused_computation.18 | convolution fusion | flops 3145728 | bytes 3156996 | tf_op jit(solution)/shard_map/dot_general | solution.py:113
  49.6 3.0 %convolution_reduce_fusion = f32[768]{0:T(1024)S(1)} fusion(bf16[768,2048]{1,0:T(8,128)(2,1)} %all-gather.7.cloned.1.call-done, bf16[2048,8]{0,1:T(8,128)(2,1)} %param.22, s32[]{:T(128)S(6)} %select_n.346), kind=kOutput, calls=%fused_computation.17 | convolution fusion | flops 3145728 | bytes 3156996 | tf_op jit(solution)/shard_map/dot_general | solution.py:113
  54.4 1.0 fusion.19
  55.6 1.0 convolution_convert_fusion.3
  57.0 13.5 %all-gather.2 = f32[4,131,256]{2,1,0:T(8,128)S(1)} all-gather(f32[1,131,256]{2,1,0:T(8,128)S(1)} %maximum_bitcast_fusion), channel_id=2, replica_groups=mesh['sp_0'=8,'sp_1'=4,'tp'=8] {'sp_1'}, dimensions={0}, use_global_device_ids=true | all-gather | bytes 670720 | tf_op jit(solution)/shard_map/all_gather | solution.py:38
  82.5 0.7 maximum_bitcast_fusion.1
  83.3 3.3 %convolution_convert_fusion = bf16[768,256]{1,0:T(8,128)(2,1)S(1)} fusion(bf16[768,2048]{1,0:T(8,128)(2,1)} %all-gather.7.cloned.1.call-done, bf16[2048,256]{1,0:T(8,128)(2,1)} %param.28), kind=kOutput, calls=%fused_computation.10 | convolution fusion | flops 805502976 | bytes 4587520 | tf_op jit(solution)/shard_map/dot_general | solution.py:113
  86.7 1.0 convolution_convert_fusion.1
  87.8 2.1 collective-permute-start
  89.9 1.0 convolution_convert_fusion.5
  90.9 1.7 convolution_convert_fusion.2
  93.8 27.6 %all-gather.9.cloned.1.call-done = f32[8,131,256]{2,1,0:T(8,128)} async-done(((f32[1,131,256]{2,1,0:T(8,128)}), f32[8,131,256]{2,1,0:T(8,128)}) %all-gather.9.cloned.1.call-update) | async-done | bytes 1073168 | tf_op jit(solution)/shard_map/all_gather | solution.py:38
  121.5 1.0 fusion.188
  144.8 0.7 fusion.194
  146.6 2.5 %multiply_reduce_fusion = (f32[768]{0:T(1024)S(1)}, f32[1,256,768]{2,1,0:T(8,128)S(1)}) fusion(f32[768]{0:T(1024)S(1)} %get-tuple-element.5, f32[1,256,768]{2,1,0:T(8,128)S(1)} %convolution_bitcast_fusion, bf16[768,128]{1,0:T(8,128)(2,1)S(1)} %convolution_convert_fusion.5, f32[8,131,256]{2,1,0:T(8,128)} %all-gather.9.cloned.1.call-done, ...), kind=kOutput, calls=%fused_computation.34 | convolution fusion | flops 305200384 | bytes 3902464 | tf_op jit(solution)/shard_map/thd,hdv->thv/dot_general | solution.py:197
  149.1 12.4 %psum.7 = f32[768]{0:T(1024)S(1)} all-reduce(f32[768]{0:T(1024)S(1)} %get-tuple-element.48), channel_id=1, replica_groups=mesh['sp_0'=8,'sp_1'=4,'tp'=8] {'tp'}, use_global_device_ids=true, to_apply=%region_8.9 | all-reduce | flops 768 | bytes 6144 | tf_op jit(solution)/shard_map/psum | solution.py:203
  161.6 1.0 fusion.12
  162.9 2.9 %add_convert_fusion = bf16[768,2048]{1,0:T(8,128)(2,1)} fusion(f32[768,2048]{1,0:T(8,128)S(1)} %fusion.12, bf16[256,2048]{1,0:T(8,128)(2,1)S(1)} %copy-done.3, f32[770,256]{1,0:T(8,128)S(1)} %maximum_convert_fusion, bf16[768,256]{1,0:T(8,128)(2,1)S(1)} %copy-done.4, f32[256]{0:T(256)S(1)} %bitcast.178, f32[256]{0:T(256)S(1)} %bitcast.177, f32[256]{0:T(256)S(1)} %bitcast.176), kind=kOutput, calls=%fused_computation | convolution fusion | flops 810024960 | bytes 13241344 | tf_op jit(solution)/shard_map/dot_general | solution.py:217
  165.8 35.1 %reduce-scatter.2.cloned.1.call-done = bf16[96,2048]{1,0:T(8,128)(2,1)} async-done(((bf16[768,2048]{1,0:T(8,128)(2,1)}), bf16[96,2048]{1,0:T(8,128)(2,1)}) %reduce-scatter.2.cloned.1.call-update) | async-done | bytes 393232 | tf_op jit(solution)/shard_map/reduce_scatter | solution.py:214
  (76 shorter events, 9.5 us)
Async XLA Ops:
  6.5 155.0 %copy-start = (bf16[256,2048]{1,0:T(8,128)(2,1)S(1)}, bf16[256,2048]{1,0:T(8,128)(2,1)}, u32[]{:S(2)}) copy-start(bf16[256,2048]{1,0:T(8,128)(2,1)} %param.32) | copy-start | bytes 3145732
  6.5 36.6 %all-gather.7.cloned.1.call-start = ((), (), s32[]{:S(2)}) async-start(), calls=%async_computation.1 | async-start | bytes 3538944 | tf_op jit(solution)/shard_map/all_gather | solution.py:111
  9.8 111.7 %all-gather.9.cloned.1.call-start = ((), (), s32[]{:S(2)}) async-start(), calls=%async_computation.3 | async-start | bytes 1253376 | tf_op jit(solution)/shard_map/all_gather | solution.py:38
  11.9 34.6 %copy-start.5 = (f32[768,1]{0,1:T(1,128)S(1)}, f32[768,1]{0,1:T(1,128)}, u32[]{:S(2)}) copy-start(f32[768,1]{0,1:T(1,128)} %param.25) | copy-start | bytes 9220
  49.6 4.8 %copy-start.1 = (bf16[768,2048]{1,0:T(8,128)(2,1)S(1)}, bf16[768,2048]{1,0:T(8,128)(2,1)}, u32[]{:S(2)}) copy-start(bf16[768,2048]{1,0:T(8,128)(2,1)} %all-gather.7.cloned.1.call-done) | copy-start | bytes 9437188
  49.6 4.8 %copy-start.9 = (bf16[2048,128]{1,0:T(8,128)(2,1)S(1)}, bf16[2048,128]{1,0:T(8,128)(2,1)}, u32[]{:S(2)}) copy-start(bf16[2048,128]{1,0:T(8,128)(2,1)} %param.20) | copy-start | bytes 1572868
  54.4 1.2 copy-start.6
  83.2 117.7 %reduce-scatter.2.cloned.1.call-start = ((), (), s32[]{:S(2)}) async-start(), calls=%async_computation.2 | async-start | bytes 3538944 | tf_op jit(solution)/shard_map/reduce_scatter | solution.py:214
  83.3 3.3 %copy-start.2 = (bf16[768,2048]{1,0:T(8,128)(2,1)S(1)}, bf16[768,2048]{1,0:T(8,128)(2,1)}, u32[]{:S(2)}) copy-start(bf16[768,2048]{1,0:T(8,128)(2,1)} %all-gather.7.cloned.1.call-done) | copy-start | bytes 9437188
  83.3 3.4 %copy-start.7 = (bf16[2048,256]{1,0:T(8,128)(2,1)S(1)}, bf16[2048,256]{1,0:T(8,128)(2,1)}, u32[]{:S(2)}) copy-start(bf16[2048,256]{1,0:T(8,128)(2,1)} %param.27) | copy-start | bytes 3145732
  86.7 3.2 %copy-start.10 = (bf16[2048,128]{1,0:T(8,128)(2,1)S(1)}, bf16[2048,128]{1,0:T(8,128)(2,1)}, u32[]{:S(2)}) copy-start(bf16[2048,128]{1,0:T(8,128)(2,1)} %param.19) | copy-start | bytes 1572868
  87.8 3.1 %copy-start.8 = (bf16[2048,256]{1,0:T(8,128)(2,1)S(1)}, bf16[2048,256]{1,0:T(8,128)(2,1)}, u32[]{:S(2)}) copy-start(bf16[2048,256]{1,0:T(8,128)(2,1)} %param.26) | copy-start | bytes 3145732
  87.8 5.9 %collective-permute-start = (bf16[2,256]{1,0:T(2,128)(2,1)S(1)}, bf16[2,256]{1,0:T(2,128)(2,1)S(1)}, u32[]{:S(2)}, u32[]{:S(2)}) collective-permute-start(bf16[2,256]{1,0:T(2,128)(2,1)S(1)} %slice.392), channel_id=1, source_target_pairs={{0,8},{8,16},{16,24},{24,32},{32,40},{40,48},{48,56},{56,64},{64,7... | collective-permute-start | bytes 3080 | tf_op jit(solution)/shard_map/ppermute | solution.py:21
  145.5 0.7 copy-start.12
  145.5 1.1 copy-start.11
  161.6 1.2 copy-start.3
  161.6 1.3 copy-start.4
Sparse Core Ops, SparseCore 0:
  9.9 33.2 all-gather.6
  83.3 38.0 all-gather.8
  165.9 34.9 reduce-scatter.1
where the time goes:
time: 208 us; the launch traced here: 207 us
  waiting for transfers between devices  94 us (45%)
  between operations  47.3 us (23%)
  blocking collectives  25.9 us (12%)
  matrix products  23.2 us (11%)
  local copies, waits for them, and re-layouts  8.19 us (4%)
  other arithmetic  6.7 us (3%)
  starting transfers between devices  2.14 us (1%)
    reduce_scatter x1, waiting for transfers between devices, per_device(): lax.psum_scatter((jnp.dot(heads_out, w_out_memory, preferred_element_type...  35.1 us
    all_gather x1, waiting for transfers between devices, per_device(): sub_rows = lax.all_gather(normed, 'tp', axis=0, tiled=True)  31.2 us
    all_gather x1, waiting for transfers between devices, collected_together(): both, at, found = (lax.all_gather(jnp.concatenate(lines), axis), 0, {})  27.6 us
    dot_general x8, matrix products, per_device(): jnp.dot(sub_rows, weight, preferred_element_type=jnp.float32)  14.8 us
    all_gather x1, blocking collectives, collected_together(): both, at, found = (lax.all_gather(jnp.concatenate(lines), axis), 0, {})  13.5 us
    psum x1, blocking collectives, per_device(): row_total = lax.psum(local_squares, 'tp')  12.4 us
  transfers between devices with their start and end apart: 4, of which 3 were waited for; matrix products, arithmetic and copies ran while one was open for 5% of the time, Pallas kernels for 0%

commit v1 on v0

--- a/solution.py
+++ b/solution.py
@@ -200,7 +200,13 @@
     denominator = jnp.sum(mixing, axis=2).T + carried * from_norm
     memory_out = numerator / jnp.maximum(jnp.abs(denominator), 1.0)[:, :, None]
     local_squares = jnp.sum(memory_out * memory_out, axis=(1, 2))
-    row_total = lax.psum(local_squares, "tp")
+    count = lax.axis_size("tp")
+    row_total, far = (local_squares, 1)
+    while far < count:
+        row_total = row_total + lax.ppermute(
+            row_total, "tp", [(i_2, i_2 ^ far) for i_2 in range(count)]
+        )
+        far = 2 * far
     row_scale = lax.rsqrt(row_total / V_WIDTH + epsilon)
     heads_out = memory_out * row_scale[:, None, None]
     heads_out = heads_out.reshape(row_count, value_width).astype(jnp.bfloat16)

time: 208 us -> 210 us (level)
  blocking collectives: 25.9 us -> 13.5 us
  waiting for transfers between devices: 94 us -> 103 us
  starting transfers between devices: 2.14 us -> 8.32 us
    psum x1 -> x0, blocking collectives: 12.4 us -> none  [per_device(): row_total = lax.psum(local_squares, 'tp')]
    ppermute x0 -> x3, starting transfers between devices: none -> 4.85 us  [per_device(): lax.ppermute(row_total, 'tp', [(i_2, i_2 ^ far) for i_2 in range(count)])]
    all_gather x1, waiting for transfers between devices: 27.6 us -> 30.8 us  [collected_together(): both, at, found = (lax.all_gather(jnp.concatenate(lines), axis), 0, {})]
    ppermute x0 -> x3, waiting for transfers between devices: none -> 3.15 us  [per_device(): lax.ppermute(row_total, 'tp', [(i_2, i_2 ^ far) for i_2 in range(count)])]
  transfers between devices with their start and end apart: 4 -> 7, of which waited for: 3 -> 5; matrix products, arithmetic and copies ran while one was open for 5% -> 4% of each run, Pallas kernels for 0% -> 0%
where the time goes in v1:
time: 210 us
  waiting for transfers between devices  103 us (49%)
  between operations  47.2 us (22%)
  matrix products  22.6 us (11%)
  blocking collectives  13.5 us (6%)
  starting transfers between devices  8.32 us (4%)
  local copies, waits for them, and re-layouts  8.08 us (4%)
  other arithmetic  6.72 us (3%)
    reduce_scatter x1, waiting for transfers between devices, per_device(): lax.psum_scatter((jnp.dot(heads_out, w_out_memory, preferred_element_type...  37 us
    all_gather x1, waiting for transfers between devices, per_device(): sub_rows = lax.all_gather(normed, 'tp', axis=0, tiled=True)  32.1 us
    all_gather x1, waiting for transfers between devices, collected_together(): both, at, found = (lax.all_gather(jnp.concatenate(lines), axis), 0, {})  30.8 us
    dot_general x8, matrix products, per_device(): jnp.dot(sub_rows, weight, preferred_element_type=jnp.float32)  14 us
    all_gather x1, blocking collectives, collected_together(): both, at, found = (lax.all_gather(jnp.concatenate(lines), axis), 0, {})  13.5 us
    ppermute x3, starting transfers between devices, per_device(): lax.ppermute(row_total, 'tp', [(i_2, i_2 ^ far) for i_2 in range(count)])  4.85 us
  transfers between devices with their start and end apart: 7, of which 5 were waited for; matrix products, arithmetic and copies ran while one was open for 4% of the time, Pallas kernels for 0%

profile of v1, /device:TPU:2, one launch (start us, length us, event | category | flops | bytes accessed | tf_op | source)
XLA Modules:
  0.0 209.6 jit_solution(14675703359749143935)
XLA Ops:
  6.5 1.3 fusion.4
  7.8 1.9 fusion.6
  9.8 1.2 dynamic_slice.13
  11.0 32.1 %all-gather.7.cloned.1.call-done = bf16[768,2048]{1,0:T(8,128)(2,1)} async-done(((bf16[96,2048]{1,0:T(8,128)(2,1)}), bf16[768,2048]{1,0:T(8,128)(2,1)}) %all-gather.7.cloned.1.call-update) | async-done | bytes 3145744 | tf_op jit(solution)/shard_map/all_gather | solution.py:111
  43.1 2.8 %convolution_reduce_fusion.1 = f32[768]{0:T(1024)S(1)} fusion(bf16[768,2048]{1,0:T(8,128)(2,1)} %all-gather.7.cloned.1.call-done, bf16[2048,8]{0,1:T(8,128)(2,1)} %param.23, s32[]{:T(128)S(6)} %select_n.346), kind=kOutput, calls=%fused_computation.18 | convolution fusion | flops 3145728 | bytes 3156996 | tf_op jit(solution)/shard_map/dot_general | solution.py:113
  49.6 3.0 %convolution_reduce_fusion = f32[768]{0:T(1024)S(1)} fusion(bf16[768,2048]{1,0:T(8,128)(2,1)} %all-gather.7.cloned.1.call-done, bf16[2048,8]{0,1:T(8,128)(2,1)} %param.22, s32[]{:T(128)S(6)} %select_n.346), kind=kOutput, calls=%fused_computation.17 | convolution fusion | flops 3145728 | bytes 3156996 | tf_op jit(solution)/shard_map/dot_general | solution.py:113
  54.4 1.0 fusion.19
  55.6 1.0 convolution_convert_fusion.3
  57.0 13.5 %all-gather.2 = f32[4,131,256]{2,1,0:T(8,128)S(1)} all-gather(f32[1,131,256]{2,1,0:T(8,128)S(1)} %maximum_bitcast_fusion), channel_id=2, replica_groups=mesh['sp_0'=8,'sp_1'=4,'tp'=8] {'sp_1'}, dimensions={0}, use_global_device_ids=true | all-gather | bytes 670720 | tf_op jit(solution)/shard_map/all_gather | solution.py:38
  84.2 3.3 %convolution_convert_fusion = bf16[768,256]{1,0:T(8,128)(2,1)S(1)} fusion(bf16[768,2048]{1,0:T(8,128)(2,1)} %all-gather.7.cloned.1.call-done, bf16[2048,256]{1,0:T(8,128)(2,1)} %param.28), kind=kOutput, calls=%fused_computation.10 | convolution fusion | flops 805502976 | bytes 4587520 | tf_op jit(solution)/shard_map/dot_general | solution.py:113
  87.6 1.0 convolution_convert_fusion.1
  89.0 1.0 convolution_convert_fusion.5
  90.0 30.8 %all-gather.9.cloned.1.call-done = f32[8,131,256]{2,1,0:T(8,128)} async-done(((f32[1,131,256]{2,1,0:T(8,128)}), f32[8,131,256]{2,1,0:T(8,128)}) %all-gather.9.cloned.1.call-update) | async-done | bytes 1073168 | tf_op jit(solution)/shard_map/all_gather | solution.py:38
  120.8 1.0 fusion.188
  146.6 2.6 %multiply_reduce_fusion = (f32[768]{0:T(1024)S(1)}, f32[1,256,768]{2,1,0:T(8,128)S(1)}) fusion(f32[768]{0:T(1024)S(1)} %get-tuple-element.5, f32[1,256,768]{2,1,0:T(8,128)S(1)} %convolution_bitcast_fusion, bf16[768,128]{1,0:T(8,128)(2,1)S(1)} %convolution_convert_fusion.5, f32[8,131,256]{2,1,0:T(8,128)} %all-gather.9.cloned.1.call-done, ...), kind=kOutput, calls=%fused_computation.34 | convolution fusion | flops 305200384 | bytes 3902464 | tf_op jit(solution)/shard_map/thd,hdv->thv/dot_general | solution.py:197
  149.5 3.4 %collective-permute-start.3 = (bf16[2,256]{1,0:T(2,128)(2,1)S(1)}, bf16[2,256]{1,0:T(2,128)(2,1)S(1)}, u32[]{:S(2)}, u32[]{:S(2)}) collective-permute-start(bf16[2,256]{1,0:T(2,128)(2,1)S(1)} %slice.392), channel_id=1, source_target_pairs={{0,8},{8,16},{16,24},{24,32},{32,40},{40,48},{48,56},{56,64},{64,7... | collective-permute-start | bytes 3080 | tf_op jit(solution)/shard_map/ppermute | solution.py:21
  152.9 1.7 collective-permute-start.1
  154.6 1.0 convolution_convert_fusion.2
  155.6 1.1 collective-permute-done.1
  156.8 3.0 %collective-permute-start.2 = (f32[768]{0:T(1024)S(1)}, f32[768]{0:T(1024)S(1)}, u32[]{:S(2)}, u32[]{:S(2)}) collective-permute-start(f32[768]{0:T(1024)S(1)} %add.433), channel_id=1, source_target_pairs={{0,4},{1,5},{2,6},{3,7},{4,0},{5,1},{6,2},{7,3},{8,12},{9,13},{10,... | collective-permute-start | bytes 9224 | tf_op jit(solution)/shard_map/ppermute | solution.py:206
  159.9 2.0 collective-permute-done.2
  161.9 1.0 fusion.12
  163.1 2.9 %add_convert_fusion = bf16[768,2048]{1,0:T(8,128)(2,1)} fusion(f32[768,2048]{1,0:T(8,128)S(1)} %fusion.12, bf16[256,2048]{1,0:T(8,128)(2,1)S(1)} %copy-done.4, f32[770,256]{1,0:T(8,128)S(1)} %maximum_convert_fusion, bf16[768,256]{1,0:T(8,128)(2,1)S(1)} %convolution_convert_fusion.2, f32[256]{0:T(256)S(1)} %bitcast.178, f32[256]{0:T(256)S(1)} %bitcast.177, ...), kind=kOutput, calls=%fused_computation | convolution fusion | flops 810024960 | bytes 13241344 | tf_op jit(solution)/shard_map/dot_general | solution.py:223
  166.0 37.0 %reduce-scatter.2.cloned.1.call-done = bf16[96,2048]{1,0:T(8,128)(2,1)} async-done(((bf16[768,2048]{1,0:T(8,128)(2,1)}), bf16[96,2048]{1,0:T(8,128)(2,1)}) %reduce-scatter.2.cloned.1.call-update) | async-done | bytes 393232 | tf_op jit(solution)/shard_map/reduce_scatter | solution.py:220
  (83 shorter events, 11.7 us)
Async XLA Ops:
  6.5 155.4 %copy-start = (bf16[256,2048]{1,0:T(8,128)(2,1)S(1)}, bf16[256,2048]{1,0:T(8,128)(2,1)}, u32[]{:S(2)}) copy-start(bf16[256,2048]{1,0:T(8,128)(2,1)} %param.32) | copy-start | bytes 3145732
  6.5 36.6 %all-gather.7.cloned.1.call-start = ((), (), s32[]{:S(2)}) async-start(), calls=%async_computation.1 | async-start | bytes 3538944 | tf_op jit(solution)/shard_map/all_gather | solution.py:111
  9.8 111.1 %all-gather.9.cloned.1.call-start = ((), (), s32[]{:S(2)}) async-start(), calls=%async_computation.3 | async-start | bytes 1253376 | tf_op jit(solution)/shard_map/all_gather | solution.py:38
  11.0 35.5 %copy-start.5 = (f32[768,1]{0,1:T(1,128)S(1)}, f32[768,1]{0,1:T(1,128)}, u32[]{:S(2)}) copy-start(f32[768,1]{0,1:T(1,128)} %param.25) | copy-start | bytes 9220
  49.6 4.8 %copy-start.1 = (bf16[768,2048]{1,0:T(8,128)(2,1)S(1)}, bf16[768,2048]{1,0:T(8,128)(2,1)}, u32[]{:S(2)}) copy-start(bf16[768,2048]{1,0:T(8,128)(2,1)} %all-gather.7.cloned.1.call-done) | copy-start | bytes 9437188
  49.6 4.8 %copy-start.9 = (bf16[2048,128]{1,0:T(8,128)(2,1)S(1)}, bf16[2048,128]{1,0:T(8,128)(2,1)}, u32[]{:S(2)}) copy-start(bf16[2048,128]{1,0:T(8,128)(2,1)} %param.20) | copy-start | bytes 1572868
  54.4 1.2 copy-start.6
  82.6 120.4 %reduce-scatter.2.cloned.1.call-start = ((), (), s32[]{:S(2)}) async-start(), calls=%async_computation.2 | async-start | bytes 3538944 | tf_op jit(solution)/shard_map/reduce_scatter | solution.py:220
  84.1 3.3 %copy-start.2 = (bf16[768,2048]{1,0:T(8,128)(2,1)S(1)}, bf16[768,2048]{1,0:T(8,128)(2,1)}, u32[]{:S(2)}) copy-start(bf16[768,2048]{1,0:T(8,128)(2,1)} %all-gather.7.cloned.1.call-done) | copy-start | bytes 9437188
  84.1 3.4 %copy-start.7 = (bf16[2048,256]{1,0:T(8,128)(2,1)S(1)}, bf16[2048,256]{1,0:T(8,128)(2,1)}, u32[]{:S(2)}) copy-start(bf16[2048,256]{1,0:T(8,128)(2,1)} %param.27) | copy-start | bytes 3145732
  87.6 1.4 copy-start.10
  145.4 0.7 copy-start.12
  145.4 1.1 copy-start.11
  146.6 8.0 %copy-start.3 = (bf16[768,2048]{1,0:T(8,128)(2,1)S(1)}, bf16[768,2048]{1,0:T(8,128)(2,1)}, u32[]{:S(2)}) copy-start(bf16[768,2048]{1,0:T(8,128)(2,1)} %all-gather.7.cloned.1.call-done) | copy-start | bytes 9437188
  146.6 8.0 %copy-start.8 = (bf16[2048,256]{1,0:T(8,128)(2,1)S(1)}, bf16[2048,256]{1,0:T(8,128)(2,1)}, u32[]{:S(2)}) copy-start(bf16[2048,256]{1,0:T(8,128)(2,1)} %param.26) | copy-start | bytes 3145732
  149.3 3.6 %collective-permute-start = (f32[768]{0:T(1024)S(1)}, f32[768]{0:T(1024)S(1)}, u32[]{:S(2)}, u32[]{:S(2)}) collective-permute-start(f32[768]{0:T(1024)S(1)} %get-tuple-element.48), channel_id=1, source_target_pairs={{0,1},{1,0},{2,3},{3,2},{4,5},{5,4},{6,7},{7,6},{8,9},{9,8},{10,11... | collective-permute-start | bytes 9224 | tf_op jit(solution)/shard_map/ppermute | solution.py:206
  149.5 10.3 %collective-permute-start.3 = (bf16[2,256]{1,0:T(2,128)(2,1)S(1)}, bf16[2,256]{1,0:T(2,128)(2,1)S(1)}, u32[]{:S(2)}, u32[]{:S(2)}) collective-permute-start(bf16[2,256]{1,0:T(2,128)(2,1)S(1)} %slice.392), channel_id=1, source_target_pairs={{0,8},{8,16},{16,24},{24,32},{32,40},{40,48},{48,56},{56,64},{64,7... | collective-permute-start | bytes 3080 | tf_op jit(solution)/shard_map/ppermute | solution.py:21
  152.9 3.9 %collective-permute-start.1 = (f32[768]{0:T(1024)S(1)}, f32[768]{0:T(1024)S(1)}, u32[]{:S(2)}, u32[]{:S(2)}) collective-permute-start(f32[768]{0:T(1024)S(1)} %add.432), channel_id=1, source_target_pairs={{0,2},{1,3},{2,0},{3,1},{4,6},{5,7},{6,4},{7,5},{8,10},{9,11},{10,... | collective-permute-start | bytes 9224 | tf_op jit(solution)/shard_map/ppermute | solution.py:206
  156.8 5.1 %collective-permute-start.2 = (f32[768]{0:T(1024)S(1)}, f32[768]{0:T(1024)S(1)}, u32[]{:S(2)}, u32[]{:S(2)}) collective-permute-start(f32[768]{0:T(1024)S(1)} %add.433), channel_id=1, source_target_pairs={{0,4},{1,5},{2,6},{3,7},{4,0},{5,1},{6,2},{7,3},{8,12},{9,13},{10,... | collective-permute-start | bytes 9224 | tf_op jit(solution)/shard_map/ppermute | solution.py:206
  161.9 1.2 copy-start.4
Sparse Core Ops, SparseCore 0:
  9.9 33.2 all-gather.6
  82.7 38.0 all-gather.8
  166.2 36.8 reduce-scatter.1
